TPU v7x, 32 devices: a whole 2x2x4 slice. The times are simulated.
32 devices in a mesh: ep: 8 (over z, x), tp: 4 (over y, core).
Axes of the slice: x: 2, y: 2, z: 4, core: 2. Of those that a mesh axis runs over, the one named last changes fastest.
Arguments:
- tokens: bfloat16 [768, 4096], P('ep'), may hold values from -6 to 6
- mix_gain: float32 [4096], replicated, may hold values from 0.1 to 1.9
- ffn_gain: float32 [4096], replicated, may hold values from 0.1 to 1.9
- in_proj: bfloat16 [4096, 1024], P(None, 'tp'), may hold values from -0.09375 to 0.09375
- decay_rate: float32 [64, 64], P('tp'), may hold values from 0.05 to 2
- frequency: float32 [64, 64], P('tp'), may hold values from -3 to 3
- log_step: float32 [64], P('tp'), may hold values from -3 to 0.5
- b_real: float32 [64, 64, 16], P('tp'), may hold values from -1.5 to 1.5
- b_imag: float32 [64, 64, 16], P('tp'), may hold values from -1.5 to 1.5
- c_real: float32 [64, 16, 64], P('tp'), may hold values from -0.75 to 0.75
- c_imag: float32 [64, 16, 64], P('tp'), may hold values from -0.75 to 0.75
- skip_gain: float32 [1024], P('tp'), may hold values from -5 to 5
- states: float32 [2, 768, 4096], P(None, 'ep', 'tp'), may hold values from -6 to 6
- out_proj: bfloat16 [1024, 4096], P('tp'), may hold values from -0.1875 to 0.1875
- route_ids: int32 [768, 2], P('ep'), may hold values from 0 to 7, all different within a row; in each aligned block of 96 rows (0 to 95, 96 to 191, ...) at most 48 rows name the same one
- route_logits: float32 [768, 2], P('ep'), may hold values from -5 to 5
- expert_gate: bfloat16 [8, 4096, 3072], P('ep', None, 'tp'), may hold values from -0.09375 to 0.09375
- expert_up: bfloat16 [8, 4096, 3072], P('ep', None, 'tp'), may hold values from -0.09375 to 0.09375
- expert_down: bfloat16 [8, 3072, 4096], P('ep', 'tp'), may hold values from -0.109375 to 0.109375
- dense_gate: bfloat16 [4096, 6144], P('tp', 'ep'), may hold values from -0.09375 to 0.09375
- dense_up: bfloat16 [4096, 6144], P('tp', 'ep'), may hold values from -0.09375 to 0.09375
- dense_down: bfloat16 [6144, 4096], P('ep', 'tp'), may hold values from -0.078125 to 0.078125
- branch_gate: bfloat16 [4096], replicated, may hold values from -0.09375 to 0.09375
Outputs:
- output: bfloat16 [768, 4096], P('ep', 'tp')
- new_states: float32 [2, 768, 4096], P(None, 'ep', 'tp')
Inputs may be any that keep to these rules, and one draw needn't show every extreme that they name: `route_ids`: each row names 2 different experts; among the rows of one device (aligned blocks of 96 rows) no expert is named by more than 48 rows.
All inputs are finite; a program needn't handle non-finite values.
Results may differ from a plain program's by a relative error of at most 0.017.
Values may be sent and summed in bfloat16 or wider, within the bound.
A program may use at most 128 MiB of HBM per device.

v0:
```python
import jax
import jax.numpy as jnp
from jax import lax
from jax.sharding import PartitionSpec as P

GROUP = 16
STATE = 64


def rms_norm(values, gain):
    flt = values.astype(jnp.float32)
    scaled = flt * lax.rsqrt(jnp.mean(flt * flt, axis=-1, keepdims=True) + 1e-06)
    return (scaled * gain).astype(jnp.bfloat16)


def discretize(decay_rate, frequency, log_step, b_real, b_imag):
    step_size = jnp.exp(log_step)[:, None]
    lam_re = -decay_rate
    magnitude = jnp.exp(lam_re * step_size)
    abar_re = magnitude * jnp.cos(frequency * step_size)
    abar_im = magnitude * jnp.sin(frequency * step_size)
    denom = lam_re * lam_re + frequency * frequency
    fac_re = ((abar_re - 1.0) * lam_re + abar_im * frequency) / denom
    fac_im = (abar_im * lam_re - (abar_re - 1.0) * frequency) / denom
    bbar_re = fac_re[..., None] * b_real - fac_im[..., None] * b_imag
    bbar_im = fac_re[..., None] * b_imag + fac_im[..., None] * b_real
    return (abar_re, abar_im, bbar_re, bbar_im)


def state_step(
    drive, states, decay_rate, frequency, log_step, b_real, b_imag, c_real, c_imag, skip_gain
):
    count = drive.shape[0]
    groups = decay_rate.shape[0]
    abar_re, abar_im, bbar_re, bbar_im = discretize(decay_rate, frequency, log_step, b_real, b_imag)
    grouped = drive.astype(jnp.float32).reshape(count, groups, GROUP)
    old_re = states[0].reshape(count, groups, STATE)
    old_im = states[1].reshape(count, groups, STATE)
    high = lax.Precision.HIGHEST
    push_re = jnp.einsum("ngh,gph->ngp", grouped, bbar_re, precision=high)
    push_im = jnp.einsum("ngh,gph->ngp", grouped, bbar_im, precision=high)
    new_re = abar_re * old_re - abar_im * old_im + push_re
    new_im = abar_re * old_im + abar_im * old_re + push_im
    readout = (
        jnp.einsum("ngp,ghp->ngh", new_re, c_real, precision=high)
        - jnp.einsum("ngp,ghp->ngh", new_im, c_imag, precision=high)
        + skip_gain.reshape(groups, GROUP) * grouped
    )
    reads = jax.nn.gelu(readout.reshape(count, groups * GROUP)).astype(jnp.bfloat16)
    fresh = jnp.stack(
        [new_re.reshape(count, groups * STATE), new_im.reshape(count, groups * STATE)]
    )
    return (reads, fresh)


def expert_rows(full_rows, gate_w, up_w, down_w, part_width):
    sources, items, width = full_rows.shape
    flat_rows = full_rows.reshape(sources * items, width)
    gate_val = jnp.dot(flat_rows, gate_w, preferred_element_type=jnp.float32)
    up_val = jnp.dot(flat_rows, up_w, preferred_element_type=jnp.float32)
    hidden = (jax.nn.silu(gate_val) * up_val).astype(jnp.bfloat16)
    partial_value = (
        jnp.dot(hidden, down_w, preferred_element_type=jnp.float32)
        .astype(jnp.bfloat16)
        .astype(jnp.float32)
    )
    summed = lax.psum_scatter(
        partial_value.astype(jnp.bfloat16), "tp", scatter_dimension=1, tiled=True
    )
    return summed.reshape(sources, items, part_width)


def shards(
    tokens,
    mix_gain,
    ffn_gain,
    in_proj,
    decay_rate,
    frequency,
    log_step,
    b_real,
    b_imag,
    c_real,
    c_imag,
    skip_gain,
    states,
    out_proj,
    route_ids,
    route_logits,
    expert_gate,
    expert_up,
    expert_down,
    dense_gate,
    dense_up,
    dense_down,
    branch_gate,
):
    seq_count, width = tokens.shape
    tp_count = lax.axis_size("tp")
    ep_count = lax.axis_size("ep")
    tp_index = lax.axis_index("tp")
    part_width = width // tp_count
    normed = rms_norm(tokens, mix_gain)
    drive = jnp.dot(normed, in_proj, preferred_element_type=jnp.float32).astype(jnp.bfloat16)
    reads, new_states = state_step(
        drive, states, decay_rate, frequency, log_step, b_real, b_imag, c_real, c_imag, skip_gain
    )
    partial_value = (
        jnp.dot(reads, out_proj, preferred_element_type=jnp.float32)
        .astype(jnp.bfloat16)
        .astype(jnp.float32)
    )
    mixed = lax.psum(partial_value.astype(jnp.bfloat16), "tp")
    resid = (tokens.astype(jnp.float32) + mixed.astype(jnp.float32)).astype(jnp.bfloat16)
    normed_two = rms_norm(resid, ffn_gain)
    own_cols = lax.dynamic_slice_in_dim(normed_two, tp_index * part_width, part_width, 1)
    hidden_width = dense_gate.shape[1]
    both_proj = jnp.concatenate([dense_gate, dense_up], axis=1)
    partial_both = jnp.dot(
        lax.all_gather(own_cols, "ep", axis=0, tiled=True),
        both_proj,
        preferred_element_type=jnp.float32,
    )
    summed_both = lax.psum(partial_both.astype(jnp.bfloat16), "tp").astype(jnp.float32)
    dense_hidden = (
        jax.nn.silu(summed_both[:, :hidden_width]) * summed_both[:, hidden_width:]
    ).astype(jnp.bfloat16)
    dense_term = lax.psum_scatter(
        jnp.dot(dense_hidden, dense_down, preferred_element_type=jnp.float32).astype(jnp.bfloat16),
        "ep",
        scatter_dimension=0,
        tiled=True,
    ).astype(jnp.float32)
    top_count = route_ids.shape[1]
    capacity = max(2, 2 * seq_count * top_count // ep_count)
    flat_ids = route_ids.reshape(-1)
    onehot = (flat_ids[:, None] == jnp.arange(ep_count, dtype=jnp.int32)[None, :]).astype(jnp.int32)
    rank = jnp.cumsum(onehot, axis=0) - onehot
    slot = jnp.sum(rank * onehot, axis=1)
    target = flat_ids * capacity + slot
    select = target[None, :] == jnp.arange(ep_count * capacity, dtype=jnp.int32)[:, None]
    select = jnp.any(select.reshape(ep_count * capacity, seq_count, top_count), axis=2).astype(
        jnp.bfloat16
    )
    send_rows = jnp.dot(select, normed_two, preferred_element_type=jnp.float32).astype(jnp.bfloat16)
    send_rows = send_rows.reshape(ep_count, capacity, width)
    send_part = lax.dynamic_slice_in_dim(send_rows, tp_index * part_width, part_width, 2)
    full_rows = lax.all_gather(
        lax.all_to_all(send_part, "ep", split_axis=0, concat_axis=0, tiled=True),
        "tp",
        axis=2,
        tiled=True,
    )
    answered = expert_rows(full_rows, expert_gate[0], expert_up[0], expert_down[0], part_width)
    returned = lax.all_to_all(answered, "ep", split_axis=0, concat_axis=0, tiled=True)
    picked_rows = returned.reshape(ep_count * capacity, part_width)[target]
    picked_rows = picked_rows.reshape(seq_count, top_count, part_width).astype(jnp.float32)
    route_weights = jax.nn.softmax(route_logits, axis=-1)
    routed = jnp.sum(route_weights[..., None] * picked_rows, axis=1)
    branch = jax.nn.sigmoid(jnp.dot(normed_two, branch_gate, preferred_element_type=jnp.float32))
    resid_cols = lax.dynamic_slice_in_dim(resid, tp_index * part_width, part_width, 1).astype(
        jnp.float32
    )
    output = (resid_cols + routed + branch[:, None] * dense_term).astype(jnp.bfloat16)
    return (output, new_states)


def solution(mesh):
    return jax.shard_map(
        shards,
        mesh=mesh,
        in_specs=(
            P("ep", None),
            P(),
            P(),
            P(None, "tp"),
            P("tp", None),
            P("tp", None),
            P("tp"),
            P("tp", None, None),
            P("tp", None, None),
            P("tp", None, None),
            P("tp", None, None),
            P("tp"),
            P(None, "ep", "tp"),
            P("tp", None),
            P("ep", None),
            P("ep", None),
            P("ep", None, "tp"),
            P("ep", None, "tp"),
            P("ep", "tp", None),
            P("tp", "ep"),
            P("tp", "ep"),
            P("ep", "tp"),
            P(),
        ),
        out_specs=(P("ep", "tp"), P(None, "ep", "tp")),
        check_vma=False,
    )
```

profile of v0, /device:TPU:0, one launch (start us, length us, event | category | flops | bytes accessed | tf_op | source)
XLA Modules:
  0.0 329.4 jit_solution(16527740815774029400)
XLA Ops:
  7.2 0.0 all-reduce.4.cloned.1.call-start
  7.2 1.4 exp.20
  8.7 2.1 fusion.69
  10.7 1.2 copy.42
  11.9 2.2 copy.43
  14.1 0.3 fusion.16
  14.4 2.8 convolution_convert_fusion.4
  17.2 0.9 copy.44
  18.1 0.8 add_divide_fusion
  18.9 1.9 fusion.26
  20.9 2.2 fusion.27
  23.1 0.1 mul.253
  23.1 1.5 fusion.70
  24.6 1.5 fusion.30
  26.1 0.1 fusion.49
  26.2 1.4 convolution_convert_fusion.1
  27.6 0.0 all-reduce.4.cloned.1.call-update
  27.6 0.0 all-gather.5.cloned.1.call-start
  27.6 0.1 copy.46
  27.7 0.1 eq.36
  27.9 37.6 %all-reduce.4.cloned.1.call-done = bf16[96,4096]{1,0:T(8,128)(2,1)} async-done(((bf16[96,4096]{1,0:T(8,128)(2,1)}), bf16[96,4096]{1,0:T(8,128)(2,1)}) %all-reduce.4.cloned.1.call-update) | async-done | bytes 786448 | tf_op jit(solution)/shard_map/psum | solution.py:113
  65.5 1.7 fusion.13
  67.3 0.9 copy-done.4
  68.1 0.3 fusion.15
  68.4 0.8 constant_dynamic-slice_fusion
  69.2 0.0 all-gather.5.cloned.1.call-update
  69.2 0.0 all-gather.3.cloned.1.call-start
  69.3 0.6 reduce-window.6
  69.9 0.2 slice_reduce_fusion
  70.1 0.1 add_bitcast_fusion
  70.3 0.6 copy-done.9
  70.8 0.8 reduce_sum.52
  71.6 0.8 broadcast_multiply_fusion
  72.4 0.1 copy.48
  72.5 0.1 fusion.41
  72.6 1.0 convolution_convert_fusion
  73.6 0.1 constant_dynamic-slice_fusion.1
  73.7 30.8 %all_to_all.10 = bf16[8,48,1024]{2,1,0:T(8,128)(2,1)} all-to-all(bf16[8,48,1024]{2,1,0:T(8,128)(2,1)S(1)} %constant_dynamic-slice_fusion.1), channel_id=1, replica_groups=mesh['ep'=8,'tp'=4] {'ep'}, dimensions={0} | all-to-all | bytes 1572864 | tf_op jit(solution)/shard_map/all_to_all | solution.py:149
  104.5 0.0 all-gather.3.cloned.1.call-update
  104.6 0.0 all-reduce.6.cloned.1.call-start
  104.6 14.9 %all-gather.5.cloned.1.call-done = bf16[768,1024]{1,0:T(8,128)(2,1)} async-done(((bf16[96,1024]{1,0:T(8,128)(2,1)}), bf16[768,1024]{1,0:T(8,128)(2,1)}) %all-gather.5.cloned.1.call-update) | async-done | bytes 1572880 | tf_op jit(solution)/shard_map/all_gather | solution.py:120
  119.5 6.4 %convolution_convert_fusion.2 = bf16[768,1536]{1,0:T(8,128)(2,1)} fusion(bf16[768,1024]{1,0:T(8,128)(2,1)} %all-gather.5.cloned.1.call-done, bf16[1024,768]{1,0:T(8,128)(2,1)} %param.43, bf16[1024,768]{1,0:T(8,128)(2,1)} %param.42), kind=kOutput, calls=%fused_computation.10 | convolution fusion | flops 2423390208 | bytes 7077888 | tf_op jit(solution)/shard_map/dot_general | solution.py:119
  125.9 0.2 reduce-scatter.3.cloned.1.call-start
  126.1 22.0 %all-gather.3.cloned.1.call-done = bf16[8,48,4096]{2,1,0:T(8,128)(2,1)} async-done(((bf16[8,48,1024]{2,1,0:T(8,128)(2,1)}), bf16[8,48,4096]{2,1,0:T(8,128)(2,1)}) %all-gather.3.cloned.1.call-update) | async-done | bytes 3145744 | tf_op jit(solution)/shard_map/all_gather | solution.py:148
  148.1 7.4 %fusion.4 = f32[384,768]{1,0:T(8,128)} fusion(bf16[384,4096]{1,0:T(8,128)(2,1)} %bitcast.89, bf16[1,4096,768]{2,1,0:T(8,128)(2,1)} %param.39), kind=kOutput, calls=%fused_computation.5 | convolution fusion | flops 2415919104 | bytes 10616832 | tf_op jit(solution)/shard_map/dot_general | solution.py:59
  155.5 14.3 %fusion.6 = bf16[384,4096]{1,0:T(8,128)(2,1)} fusion(bf16[1,768,4096]{2,1,0:T(8,128)(2,1)} %param.41, bf16[384,4096]{1,0:T(8,128)(2,1)} %bitcast.90, bf16[1,4096,768]{2,1,0:T(8,128)(2,1)} %param.40, f32[384,768]{1,0:T(8,128)} %fusion.4), kind=kOutput, calls=%fused_computation.8 | convolution fusion | flops 4835180544 | bytes 20054016 | tf_op jit(solution)/shard_map/dot_general | solution.py:63
  169.8 0.0 reduce-scatter.5.cloned.1.call-start
  169.9 36.2 %all-reduce.6.cloned.1.call-done = bf16[768,1536]{1,0:T(8,128)(2,1)} async-done(((bf16[768,1536]{1,0:T(8,128)(2,1)}), bf16[768,1536]{1,0:T(8,128)(2,1)}) %all-reduce.6.cloned.1.call-update) | async-done | bytes 2359312 | tf_op jit(solution)/shard_map/psum | solution.py:124
  206.0 2.4 convert_element_type.91
  208.5 2.6 convolution_convert_fusion.3
  211.1 35.2 %reduce-scatter.3.cloned.1.call-done = bf16[384,1024]{1,0:T(8,128)(2,1)} async-done(((bf16[384,4096]{1,0:T(8,128)(2,1)}), bf16[384,1024]{1,0:T(8,128)(2,1)}) %reduce-scatter.3.cloned.1.call-update) | async-done | bytes 786448 | tf_op jit(solution)/shard_map/reduce_scatter | solution.py:67
  246.2 5.5 %all-to-all-start.1 = ((bf16[8,48,1024]{2,1,0:T(8,128)(2,1)}), bf16[8,48,1024]{2,1,0:T(8,128)(2,1)S(1)}, u32[]{:S(2)}, u32[]{:S(2)}) async-start(bf16[8,48,1024]{2,1,0:T(8,128)(2,1)} %bitcast.86), calls=%async_computation.2 | async-start | bytes 1572864 | tf_op jit(solution)/shard_map/all_to_all | solution.py:155
  251.8 0.1 mul.275
  252.0 0.1 copy.45
  252.1 2.0 copy.50
  254.1 0.9 copy.49
  255.0 2.1 pad_maximum_fusion
  257.1 1.4 fusion.34
  258.5 22.2 %all-to-all-done.1 = bf16[8,48,1024]{2,1,0:T(8,128)(2,1)S(1)} async-done(((bf16[8,48,1024]{2,1,0:T(8,128)(2,1)}), bf16[8,48,1024]{2,1,0:T(8,128)(2,1)S(1)}, u32[]{:S(2)}, u32[]{:S(2)}) %all-to-all-start.1) | async-done | bytes 786464 | tf_op jit(solution)/shard_map/all_to_all | solution.py:155
  280.8 1.0 gather_fusion
  281.8 0.5 reshape.124
  282.3 1.0 multiply_reduce_fusion
  283.3 37.4 %reduce-scatter.5.cloned.1.call-done = bf16[96,1024]{1,0:T(8,128)(2,1)} async-done(((bf16[768,1024]{1,0:T(8,128)(2,1)}), bf16[96,1024]{1,0:T(8,128)(2,1)}) %reduce-scatter.5.cloned.1.call-update) | async-done | bytes 196624 | tf_op jit(solution)/shard_map/reduce_scatter | solution.py:128
  320.7 1.8 add_convert_fusion
  (50 shorter events, 0.3 us)
Async XLA Ops:
  7.2 19.0 %copy-start = (bf16[256,4096]{1,0:T(8,128)(2,1)S(1)}, bf16[256,4096]{1,0:T(8,128)(2,1)}, u32[]{:S(2)}) copy-start(bf16[256,4096]{1,0:T(8,128)(2,1)} %param.36) | copy-start | bytes 6291460
  7.2 6.9 %copy-start.5 = (bf16[96,4096]{1,0:T(8,128)(2,1)S(1)}, bf16[96,4096]{1,0:T(8,128)(2,1)}, u32[]{:S(2)}) copy-start(bf16[96,4096]{1,0:T(8,128)(2,1)} %param.23) | copy-start | bytes 2359300
  7.2 58.3 %all-reduce.4.cloned.1.call-start = ((), (), s32[]{:S(2)}) async-start(), calls=%async_computation.4 | async-start | bytes 1572864 | tf_op jit(solution)/shard_map/psum | solution.py:113
  11.9 7.0 %copy-start.2 = (f32[1,96,1024]{1,2,0:T(8,128)}, f32[1,96,1024]{1,2,0:T(8,128)S(1)}, u32[]{:S(2)}) copy-start(f32[1,96,1024]{1,2,0:T(8,128)S(1)} %copy.42) | copy-start | bytes 1179652
  14.1 4.0 %copy-start.12 = (f32[16,64]{1,0:T(8,128)S(1)}, f32[16,64]{1,0:T(8,128)}, u32[]{:S(2)}) copy-start(f32[16,64]{1,0:T(8,128)} %param.28) | copy-start | bytes 12292
  14.1 4.0 %copy-start.13 = (f32[16,64]{1,0:T(8,128)S(1)}, f32[16,64]{1,0:T(8,128)}, u32[]{:S(2)}) copy-start(f32[16,64]{1,0:T(8,128)} %param.27) | copy-start | bytes 12292
  14.1 4.8 %copy-start.6 = (f32[16,64,16]{1,2,0:T(8,128)S(1)}, f32[16,64,16]{1,2,0:T(8,128)}, u32[]{:S(2)}) copy-start(f32[16,64,16]{1,2,0:T(8,128)} %param.31) | copy-start | bytes 196612
  17.1 3.7 %copy-start.7 = (f32[16,64,16]{1,2,0:T(8,128)S(1)}, f32[16,64,16]{1,2,0:T(8,128)}, u32[]{:S(2)}) copy-start(f32[16,64,16]{1,2,0:T(8,128)} %param.30) | copy-start | bytes 196612
  17.2 5.9 %copy-start.15 = (f32[256]{0:T(256)S(1)}, f32[256]{0:T(256)}, u32[]{:S(2)}) copy-start(f32[256]{0:T(256)} %param.34) | copy-start | bytes 3076
  20.9 6.7 %copy-start.1 = (f32[96,16,64]{0,2,1:T(8,128)}, f32[96,16,64]{0,2,1:T(8,128)S(1)}, u32[]{:S(2)}) copy-start(f32[96,16,64]{0,2,1:T(8,128)S(1)} %fusion.26) | copy-start | bytes 1179652
  26.1 1.5 copy-start.16
  27.5 40.6 %copy-start.8 = (f32[4096]{0:T(1024)S(1)}, f32[4096]{0:T(1024)}, u32[]{:S(2)}) copy-start(f32[4096]{0:T(1024)} %param.25) | copy-start | bytes 49156
  27.6 91.9 %all-gather.5.cloned.1.call-start = ((), (), s32[]{:S(2)}) async-start(), calls=%async_computation.7 | async-start | bytes 1769472 | tf_op jit(solution)/shard_map/all_gather | solution.py:120
  67.2 0.9 copy-start.4
  68.4 5.2 %copy-start.3 = (bf16[96,4096]{1,0:T(8,128)(2,1)}, bf16[96,4096]{1,0:T(8,128)(2,1)S(1)}, u32[]{:S(2)}) copy-start(bf16[96,4096]{1,0:T(8,128)(2,1)S(1)} %fusion.15) | copy-start | bytes 2359300
  69.2 78.9 %all-gather.3.cloned.1.call-start = ((), (), s32[]{:S(2)}) async-start(), calls=%async_computation.5 | async-start | bytes 3932160 | tf_op jit(solution)/shard_map/all_gather | solution.py:148
  70.3 0.6 copy-start.9
  104.6 101.5 %all-reduce.6.cloned.1.call-start = ((), (), s32[]{:S(2)}) async-start(), calls=%async_computation.8 | async-start | bytes 4718592 | tf_op jit(solution)/shard_map/psum | solution.py:124
  125.9 120.4 %reduce-scatter.3.cloned.1.call-start = ((), (), s32[]{:S(2)}) async-start(), calls=%async_computation.6 | async-start | bytes 3932160 | tf_op jit(solution)/shard_map/reduce_scatter | solution.py:67
  169.8 150.9 %reduce-scatter.5.cloned.1.call-start = ((), (), s32[]{:S(2)}) async-start(), calls=%async_computation.9 | async-start | bytes 1769472 | tf_op jit(solution)/shard_map/reduce_scatter | solution.py:128
  206.0 2.4 copy-start.17
  211.0 40.9 %copy-start.11 = (f32[96,2]{0,1:T(2,128)S(1)}, f32[96,2]{0,1:T(2,128)}, u32[]{:S(2)}) copy-start(f32[96,2]{0,1:T(2,128)} %param.38) | copy-start | bytes 2308
  211.0 41.0 %copy-start.14 = (bf16[4096]{0:T(1024)(128)(2,1)S(1)}, bf16[4096]{0:T(1024)(128)(2,1)}, u32[]{:S(2)}) copy-start(bf16[4096]{0:T(1024)(128)(2,1)} %param.45) | copy-start | bytes 24580
  211.1 43.9 %copy-start.10 = (s32[192]{0:T(256)S(1)}, s32[192]{0:T(256)}, u32[]{:S(2)}) copy-start(s32[192]{0:T(256)} %copy-done.9) | copy-start | bytes 2308
  246.2 34.5 %all-to-all-start.1 = ((bf16[8,48,1024]{2,1,0:T(8,128)(2,1)}), bf16[8,48,1024]{2,1,0:T(8,128)(2,1)S(1)}, u32[]{:S(2)}, u32[]{:S(2)}) async-start(bf16[8,48,1024]{2,1,0:T(8,128)(2,1)} %bitcast.86), calls=%async_computation.2 | async-start | bytes 1572864 | tf_op jit(solution)/shard_map/all_to_all | solution.py:155
Sparse Core Ops, SparseCore 0:
  27.7 37.7 all-reduce.3
  69.3 50.0 all-gather.4
  121.0 27.0 all-gather.2
  150.3 55.6 all-reduce.5
  208.4 37.7 reduce-scatter.2
  249.5 71.1 reduce-scatter.4
where the time goes:
time: 330 us; the launch traced here: 329 us
  waiting for transfers between devices  205 us (62%)
  matrix products  44.3 us (13%)
  blocking collectives  30.8 us (9%)
  local copies, waits for them, and re-layouts  16.2 us (5%)
  between operations  14.4 us (4%)
  other arithmetic  12.1 us (4%)
  starting transfers between devices  5.94 us (2%)
    psum x1, waiting for transfers between devices, shards(): mixed = lax.psum(partial_value.astype(jnp.bfloat16), 'tp')  37.6 us
    reduce_scatter x1, waiting for transfers between devices, shards(): lax.psum_scatter(jnp.dot(dense_hidden, dense_down, preferred_element_type...  37.4 us
    psum x1, waiting for transfers between devices, shards(): lax.psum(partial_both.astype(jnp.bfloat16), 'tp').astype(jnp.float32)  36.2 us
    reduce_scatter x1, waiting for transfers between devices, expert_rows(): lax.psum_scatter(partial_value.astype(jnp.bfloat16), 'tp', scatter_dimens...  35.2 us
    all_to_all x1, blocking collectives, shards(): lax.all_to_all(send_part, 'ep', split_axis=0, concat_axis=0, tiled=True)  30.8 us
    all_to_all x1, waiting for transfers between devices, shards(): lax.all_to_all(answered, 'ep', split_axis=0, concat_axis=0, tiled=True)  22.2 us
    all_gather x1, waiting for transfers between devices, shards(): lax.all_gather(lax.all_to_all(send_part, 'ep', split_axis=0, concat_axis=...  22 us
    all_gather x1, waiting for transfers between devices, shards(): lax.all_gather(own_cols, 'ep', axis=0, tiled=True)  14.9 us
  transfers between devices with their start and end apart: 7, of which 7 were waited for; matrix products, arithmetic and copies ran while one was open for 14% of the time, Pallas kernels for 0%

commit v1 on v0

--- a/solution.py
+++ b/solution.py
@@ -5,6 +5,19 @@
 
 GROUP = 16
 STATE = 64
+
+
+def ring_gather(x, axis, dim):
+    ways = lax.axis_size(axis)
+    up = [(d, (d + 1) % ways) for d in range(ways)]
+    down = [(d, (d - 1) % ways) for d in range(ways)]
+    earlier, later = ([x], [x])
+    for _ in range(ways // 2):
+        earlier.append(lax.ppermute(earlier[-1], axis, up))
+    for _ in range((ways - 1) // 2):
+        later.append(lax.ppermute(later[-1], axis, down))
+    line = jnp.concatenate([*earlier[::-1], *later[1:]], axis=dim)
+    return jnp.roll(line, (lax.axis_index(axis) - ways // 2) * x.shape[dim], axis=dim)
 
 
 def rms_norm(values, gain):
@@ -145,11 +158,8 @@
     send_rows = jnp.dot(select, normed_two, preferred_element_type=jnp.float32).astype(jnp.bfloat16)
     send_rows = send_rows.reshape(ep_count, capacity, width)
     send_part = lax.dynamic_slice_in_dim(send_rows, tp_index * part_width, part_width, 2)
-    full_rows = lax.all_gather(
-        lax.all_to_all(send_part, "ep", split_axis=0, concat_axis=0, tiled=True),
-        "tp",
-        axis=2,
-        tiled=True,
+    full_rows = ring_gather(
+        lax.all_to_all(send_part, "ep", split_axis=0, concat_axis=0, tiled=True), "tp", 2
     )
     answered = expert_rows(full_rows, expert_gate[0], expert_up[0], expert_down[0], part_width)
     returned = lax.all_to_all(answered, "ep", split_axis=0, concat_axis=0, tiled=True)

time: 330 us -> 298 us (0.903)
  waiting for transfers between devices: 205 us -> 179 us
  matrix products: 44.3 us -> 40.5 us
    all_gather x1 -> x0, waiting for transfers between devices: 22 us -> none  [shards(): lax.all_gather(lax.all_to_all(send_part, 'ep', split_axis=0, concat_axis=...]
    ppermute x0 -> x3, waiting for transfers between devices: none -> 18.3 us  [the longest x2 16.9 us: ring_gather(): earlier.append(lax.ppermute(earlier[-1], axis, up))]
    psum x1, waiting for transfers between devices: 36.2 us -> 21.4 us  [shards(): lax.psum(partial_both.astype(jnp.bfloat16), 'tp').astype(jnp.float32)]
    all_gather x1, waiting for transfers between devices: 14.9 us -> 4.76 us  [shards(): lax.all_gather(own_cols, 'ep', axis=0, tiled=True)]
    all_to_all x1, waiting for transfers between devices: 22.2 us -> 27 us  [shards(): lax.all_to_all(answered, 'ep', split_axis=0, concat_axis=0, tiled=True)]
    unnamed x38 -> x45, local copies, waits for them, and re-layouts: 1.64 us -> 6.04 us
    dot_general x1, matrix products: 7.36 us -> 3.61 us  [expert_rows(): up_val = jnp.dot(flat_rows, up_w, preferred_element_type=jnp.float32)]
  transfers between devices with their start and end apart: 7 -> 9, of which waited for: 7 -> 9; matrix products, arithmetic and copies ran while one was open for 14% -> 15% of each run, Pallas kernels for 0% -> 0%
where the time goes in v1:
time: 298 us; the launch traced here: 297 us
  waiting for transfers between devices  179 us (60%)
  matrix products  40.5 us (14%)
  blocking collectives  30.7 us (10%)
  local copies, waits for them, and re-layouts  14.5 us (5%)
  between operations  14.2 us (5%)
  other arithmetic  10.6 us (4%)
  starting transfers between devices  7.65 us (3%)
    reduce_scatter x1, waiting for transfers between devices, shards(): lax.psum_scatter(jnp.dot(dense_hidden, dense_down, preferred_element_type...  37.4 us
    psum x1, waiting for transfers between devices, shards(): mixed = lax.psum(partial_value.astype(jnp.bfloat16), 'tp')  36.3 us
    reduce_scatter x1, waiting for transfers between devices, expert_rows(): lax.psum_scatter(partial_value.astype(jnp.bfloat16), 'tp', scatter_dimens...  33.9 us
    all_to_all x1, blocking collectives, shards(): lax.all_to_all(send_part, 'ep', split_axis=0, concat_axis=0, tiled=True)  30.7 us
    all_to_all x1, waiting for transfers between devices, shards(): lax.all_to_all(answered, 'ep', split_axis=0, concat_axis=0, tiled=True)  27 us
    psum x1, waiting for transfers between devices, shards(): lax.psum(partial_both.astype(jnp.bfloat16), 'tp').astype(jnp.float32)  21.4 us
    ppermute x2, waiting for transfers between devices, ring_gather(): earlier.append(lax.ppermute(earlier[-1], axis, up))  16.9 us
    dot_general x1, matrix products, expert_rows(): jnp.dot(hidden, down_w, preferred_element_type=jnp.float32)  14.3 us
  transfers between devices with their start and end apart: 9, of which 9 were waited for; matrix products, arithmetic and copies ran while one was open for 15% of the time, Pallas kernels for 0%

profile of v1, /device:TPU:0, one launch (start us, length us, event | category | flops | bytes accessed | tf_op | source)
XLA Modules:
  0.0 297.3 jit_solution(15868998011968337983)
XLA Ops:
  7.2 0.8 exp.20
  8.0 1.4 fusion.16
  9.4 2.4 convolution_convert_fusion.4
  11.8 0.1 copy.44
  12.0 1.2 fusion.65
  13.1 0.2 copy.42
  13.4 1.0 copy.43
  14.4 0.1 add_divide_fusion
  14.5 2.0 fusion.20
  16.5 2.2 fusion.21
  18.7 0.1 mul.256
  18.8 1.5 fusion.66
  20.3 1.5 fusion.24
  21.8 1.4 convolution_convert_fusion.1
  23.3 0.1 copy.46
  23.4 0.1 eq.39
  23.6 0.6 reduce-window.6
  24.2 0.2 slice_reduce_fusion
  24.4 0.1 add_bitcast_fusion
  24.5 0.1 reduce_sum.52
  24.7 0.1 copy.48
  24.7 0.1 fusion.37
  24.9 36.3 %all-reduce.4.cloned.1.call-done = bf16[96,4096]{1,0:T(8,128)(2,1)} async-done(((bf16[96,4096]{1,0:T(8,128)(2,1)}), bf16[96,4096]{1,0:T(8,128)(2,1)}) %all-reduce.4.cloned.1.call-update) | async-done | bytes 786448 | tf_op jit(solution)/shard_map/psum | solution.py:126
  61.1 1.7 fusion.13
  62.9 0.3 fusion.15
  63.2 0.7 constant_dynamic-slice_fusion
  64.0 1.0 convolution_convert_fusion
  65.0 0.1 constant_dynamic-slice_fusion.2
  65.1 30.7 %all_to_all.10 = bf16[8,48,1024]{2,1,0:T(8,128)(2,1)S(1)} all-to-all(bf16[8,48,1024]{2,1,0:T(8,128)(2,1)S(1)} %constant_dynamic-slice_fusion.2), channel_id=1, replica_groups=mesh['ep'=8,'tp'=4] {'ep'}, dimensions={0} | all-to-all | bytes 1572864 | tf_op jit(solution)/shard_map/all_to_all | solution.py:162
  95.7 11.4 %collective-permute-done = bf16[8,48,1024]{2,1,0:T(8,128)(2,1)S(1)} collective-permute-done((bf16[8,48,1024]{2,1,0:T(8,128)(2,1)S(1)}, bf16[8,48,1024]{2,1,0:T(8,128)(2,1)S(1)}, u32[]{:S(2)}, u32[]{:S(2)}) %collective-permute-start) | collective-permute-done | bytes 786464 | tf_op jit(solution)/shard_map/ppermute | solution.py:16
  107.2 1.7 collective-permute-start.2
  108.9 4.8 %all-gather.2.cloned.1.call-done = bf16[768,1024]{1,0:T(8,128)(2,1)} async-done(((bf16[96,1024]{1,0:T(8,128)(2,1)}), bf16[768,1024]{1,0:T(8,128)(2,1)}) %all-gather.2.cloned.1.call-update) | async-done | bytes 1572880 | tf_op jit(solution)/shard_map/all_gather | solution.py:133
  113.7 6.4 %convolution_convert_fusion.2 = bf16[768,1536]{1,0:T(8,128)(2,1)} fusion(bf16[768,1024]{1,0:T(8,128)(2,1)} %all-gather.2.cloned.1.call-done, bf16[1024,768]{1,0:T(8,128)(2,1)} %param.43, bf16[1024,768]{1,0:T(8,128)(2,1)} %param.42), kind=kOutput, calls=%fused_computation.10 | convolution fusion | flops 2423390208 | bytes 7077888 | tf_op jit(solution)/shard_map/dot_general | solution.py:132
  120.1 0.2 reduce-scatter.3.cloned.1.call-start
  120.3 5.5 %collective-permute-done.1 = bf16[8,48,1024]{2,1,0:T(8,128)(2,1)} collective-permute-done((bf16[8,48,1024]{2,1,0:T(8,128)(2,1)S(1)}, bf16[8,48,1024]{2,1,0:T(8,128)(2,1)}, u32[]{:S(2)}, u32[]{:S(2)}) %collective-permute-start.1) | collective-permute-done | bytes 786464 | tf_op jit(solution)/shard_map/ppermute | solution.py:16
  125.8 1.2 constant_dynamic-update-slice_fusion.7
  127.0 0.1 constant_dynamic-update-slice_fusion.6
  127.1 0.1 constant_dynamic-update-slice_fusion.5
  127.1 1.4 collective-permute-done.2
  128.5 1.3 constant_dynamic-update-slice_fusion.4
  129.9 1.4 constant_dynamic-update-slice_fusion.3
  131.3 0.1 constant_dynamic-update-slice_fusion.2
  131.4 1.3 constant_dynamic-update-slice_fusion
  132.8 0.3 constant_dynamic-slice_fusion.1
  133.1 1.7 copy-done.6
  134.8 3.6 %fusion.2 = f32[384,768]{1,0:T(8,128)} fusion(bf16[384,4096]{1,0:T(8,128)(2,1)S(1)} %bitcast.81, bf16[1,4096,768]{2,1,0:T(8,128)(2,1)S(1)} %bitcast.90), kind=kOutput, calls=%fused_computation.3 | convolution fusion | flops 2415919104 | bytes 10616832 | tf_op jit(solution)/shard_map/dot_general | solution.py:73
  138.4 14.3 %fusion.6 = bf16[384,4096]{1,0:T(8,128)(2,1)} fusion(bf16[1,768,4096]{2,1,0:T(8,128)(2,1)} %param.41, f32[384,768]{1,0:T(8,128)} %fusion.2, bf16[384,4096]{1,0:T(8,128)(2,1)} %bitcast.82, bf16[1,4096,768]{2,1,0:T(8,128)(2,1)} %param.39), kind=kOutput, calls=%fused_computation.8 | convolution fusion | flops 4835180544 | bytes 20054016 | tf_op jit(solution)/shard_map/dot_general | solution.py:76
  152.8 21.4 %all-reduce.6.cloned.1.call-done = bf16[768,1536]{1,0:T(8,128)(2,1)} async-done(((bf16[768,1536]{1,0:T(8,128)(2,1)}), bf16[768,1536]{1,0:T(8,128)(2,1)}) %all-reduce.6.cloned.1.call-update) | async-done | bytes 2359312 | tf_op jit(solution)/shard_map/psum | solution.py:137
  174.3 2.3 convert_element_type.91
  176.6 4.0 %convolution_convert_fusion.3 = bf16[768,1024]{1,0:T(8,128)(2,1)} fusion(bf16[768,1024]{1,0:T(8,128)(2,1)} %param.44, f32[768,1536]{1,0:T(8,128)S(1)} %convert_element_type.91), kind=kOutput, calls=%fused_computation.21 | convolution fusion | flops 1212284928 | bytes 7864320 | tf_op jit(solution)/shard_map/dot_general | solution.py:142
  180.6 33.9 %reduce-scatter.3.cloned.1.call-done = bf16[384,1024]{1,0:T(8,128)(2,1)} async-done(((bf16[384,4096]{1,0:T(8,128)(2,1)}), bf16[384,1024]{1,0:T(8,128)(2,1)}) %reduce-scatter.3.cloned.1.call-update) | async-done | bytes 786448 | tf_op jit(solution)/shard_map/reduce_scatter | solution.py:80
  214.5 5.5 %all-to-all-start.1 = ((bf16[8,48,1024]{2,1,0:T(8,128)(2,1)}), bf16[8,48,1024]{2,1,0:T(8,128)(2,1)S(1)}, u32[]{:S(2)}, u32[]{:S(2)}) async-start(bf16[8,48,1024]{2,1,0:T(8,128)(2,1)} %bitcast.86), calls=%async_computation.2 | async-start | bytes 1572864 | tf_op jit(solution)/shard_map/all_to_all | solution.py:165
  220.1 0.1 copy.45
  220.2 0.1 mul.279
  220.3 0.2 copy.50
  220.5 0.2 copy.49
  220.8 1.0 pad_maximum_fusion
  221.7 0.3 fusion.28
  222.0 27.0 %all-to-all-done.1 = bf16[8,48,1024]{2,1,0:T(8,128)(2,1)S(1)} async-done(((bf16[8,48,1024]{2,1,0:T(8,128)(2,1)}), bf16[8,48,1024]{2,1,0:T(8,128)(2,1)S(1)}, u32[]{:S(2)}, u32[]{:S(2)}) %all-to-all-start.1) | async-done | bytes 786464 | tf_op jit(solution)/shard_map/all_to_all | solution.py:165
  249.0 1.0 gather_fusion
  250.0 0.5 reshape.124
  250.5 1.0 multiply_reduce_fusion
  251.6 37.4 %reduce-scatter.5.cloned.1.call-done = bf16[96,1024]{1,0:T(8,128)(2,1)} async-done(((bf16[768,1024]{1,0:T(8,128)(2,1)}), bf16[96,1024]{1,0:T(8,128)(2,1)}) %reduce-scatter.5.cloned.1.call-update) | async-done | bytes 196624 | tf_op jit(solution)/shard_map/reduce_scatter | solution.py:141
  288.9 1.8 add_convert_fusion
  (63 shorter events, 0.6 us)
Async XLA Ops:
  7.2 14.7 %copy-start = (bf16[256,4096]{1,0:T(8,128)(2,1)S(1)}, bf16[256,4096]{1,0:T(8,128)(2,1)}, u32[]{:S(2)}) copy-start(bf16[256,4096]{1,0:T(8,128)(2,1)} %param.36) | copy-start | bytes 6291460
  7.2 54.0 %all-reduce.4.cloned.1.call-start = ((), (), s32[]{:S(2)}) async-start(), calls=%async_computation.4 | async-start | bytes 1572864 | tf_op jit(solution)/shard_map/psum | solution.py:126
  11.8 2.6 copy-start.11
  11.8 2.6 copy-start.12
  13.3 1.2 copy-start.4
  13.3 3.2 %copy-start.7 = (f32[16,64,16]{1,2,0:T(8,128)S(1)}, f32[16,64,16]{1,2,0:T(8,128)}, u32[]{:S(2)}) copy-start(f32[16,64,16]{1,2,0:T(8,128)} %param.31) | copy-start | bytes 196612
  13.4 3.1 %copy-start.8 = (f32[16,64,16]{1,2,0:T(8,128)S(1)}, f32[16,64,16]{1,2,0:T(8,128)}, u32[]{:S(2)}) copy-start(f32[16,64,16]{1,2,0:T(8,128)} %param.30) | copy-start | bytes 196612
  13.4 5.3 %copy-start.14 = (f32[256]{0:T(256)S(1)}, f32[256]{0:T(256)}, u32[]{:S(2)}) copy-start(f32[256]{0:T(256)} %param.34) | copy-start | bytes 3076
  16.5 6.7 %copy-start.2 = (f32[96,16,64]{0,2,1:T(8,128)}, f32[96,16,64]{0,2,1:T(8,128)S(1)}, u32[]{:S(2)}) copy-start(f32[96,16,64]{0,2,1:T(8,128)S(1)} %fusion.20) | copy-start | bytes 1179652
  20.3 3.0 %copy-start.15 = (s32[96,2]{0,1:T(2,128)S(1)}, s32[96,2]{0,1:T(2,128)}, u32[]{:S(2)}) copy-start(s32[96,2]{0,1:T(2,128)} %param.37) | copy-start | bytes 2308
  23.2 39.7 %copy-start.9 = (f32[4096]{0:T(1024)S(1)}, f32[4096]{0:T(1024)}, u32[]{:S(2)}) copy-start(f32[4096]{0:T(1024)} %param.25) | copy-start | bytes 49156
  23.2 90.4 %all-gather.2.cloned.1.call-start = ((), (), s32[]{:S(2)}) async-start(), calls=%async_computation.6 | async-start | bytes 1769472 | tf_op jit(solution)/shard_map/all_gather | solution.py:133
  62.9 2.1 copy-start.5
  63.9 110.3 %all-reduce.6.cloned.1.call-start = ((), (), s32[]{:S(2)}) async-start(), calls=%async_computation.7 | async-start | bytes 4718592 | tf_op jit(solution)/shard_map/psum | solution.py:137
  95.7 11.4 %collective-permute-start = (bf16[8,48,1024]{2,1,0:T(8,128)(2,1)S(1)}, bf16[8,48,1024]{2,1,0:T(8,128)(2,1)S(1)}, u32[]{:S(2)}, u32[]{:S(2)}) collective-permute-start(bf16[8,48,1024]{2,1,0:T(8,128)(2,1)S(1)} %all_to_all.10), channel_id=1, source_target_pairs={{0,1},{1,2},{2,3},{3,0},{4,5},{5,6},{6,7},{7,4},{8,9},{9,10},{10,1... | collective-permute-start | bytes 2359304 | tf_op jit(solution)/shard_map/ppermute | solution.py:16
  107.2 18.6 %collective-permute-start.1 = (bf16[8,48,1024]{2,1,0:T(8,128)(2,1)S(1)}, bf16[8,48,1024]{2,1,0:T(8,128)(2,1)}, u32[]{:S(2)}, u32[]{:S(2)}) collective-permute-start(bf16[8,48,1024]{2,1,0:T(8,128)(2,1)S(1)} %collective-permute-done), channel_id=1, source_target_pairs={{0,1},{1,2},{2,3},{3,0},{4,5},{5,6},{6,7},{7,4},{8,9},{9,10},{10,1... | collective-permute-start | bytes 2359304 | tf_op jit(solution)/shard_map/ppermute | solution.py:16
  107.2 21.4 %collective-permute-start.2 = (bf16[8,48,1024]{2,1,0:T(8,128)(2,1)S(1)}, bf16[8,48,1024]{2,1,0:T(8,128)(2,1)}, u32[]{:S(2)}, u32[]{:S(2)}) collective-permute-start(bf16[8,48,1024]{2,1,0:T(8,128)(2,1)S(1)} %all_to_all.10), channel_id=1, source_target_pairs={{0,3},{1,0},{2,1},{3,2},{4,7},{5,4},{6,5},{7,6},{8,11},{9,8},{10,9... | collective-permute-start | bytes 2359304 | tf_op jit(solution)/shard_map/ppermute | solution.py:18
  120.1 94.4 %reduce-scatter.3.cloned.1.call-start = ((), (), s32[]{:S(2)}) async-start(), calls=%async_computation.5 | async-start | bytes 3932160 | tf_op jit(solution)/shard_map/reduce_scatter | solution.py:80
  128.5 6.3 %slice-start = ((s8[6291456]{0:T(1024)(128)(4,1)}), s8[4194304]{0:T(1024)(128)(4,1)S(1)}, s32[]{:S(2)}) async-start(s8[6291456]{0:T(1024)(128)(4,1)} %bitcast.89), calls=%async_computation.9 | async-start | bytes 8388608
  131.4 3.4 %slice-start.1 = ((s8[6291456]{0:T(1024)(128)(4,1)}), s8[2097152]{0:T(1024)(128)(4,1)S(1)}, s32[]{:S(2)}) async-start(s8[6291456]{0:T(1024)(128)(4,1)} %bitcast.89), calls=%async_computation.10 | async-start | bytes 4194304
  133.1 1.7 copy-start.6
  152.8 136.2 %reduce-scatter.5.cloned.1.call-start = ((), (), s32[]{:S(2)}) async-start(), calls=%async_computation.8 | async-start | bytes 1769472 | tf_op jit(solution)/shard_map/reduce_scatter | solution.py:141
  180.6 39.4 %copy-start.13 = (bf16[4096]{0:T(1024)(128)(2,1)S(1)}, bf16[4096]{0:T(1024)(128)(2,1)}, u32[]{:S(2)}) copy-start(bf16[4096]{0:T(1024)(128)(2,1)} %param.45) | copy-start | bytes 24580
  180.6 39.4 %copy-start.10 = (f32[96,2]{0,1:T(2,128)S(1)}, f32[96,2]{0,1:T(2,128)}, u32[]{:S(2)}) copy-start(f32[96,2]{0,1:T(2,128)} %param.38) | copy-start | bytes 2308
  180.6 39.8 %copy-start.3 = (f32[96,16,64]{0,2,1:T(8,128)S(1)}, f32[96,16,64]{0,2,1:T(8,128)}, u32[]{:S(2)}) copy-start(f32[96,16,64]{0,2,1:T(8,128)} %copy-done.2) | copy-start | bytes 1179652
  214.5 34.5 %all-to-all-start.1 = ((bf16[8,48,1024]{2,1,0:T(8,128)(2,1)}), bf16[8,48,1024]{2,1,0:T(8,128)(2,1)S(1)}, u32[]{:S(2)}, u32[]{:S(2)}) async-start(bf16[8,48,1024]{2,1,0:T(8,128)(2,1)} %bitcast.86), calls=%async_computation.2 | async-start | bytes 1572864 | tf_op jit(solution)/shard_map/all_to_all | solution.py:165
  249.0 41.7 %copy-start.1 = (bf16[256,4096]{1,0:T(8,128)(2,1)S(1)}, bf16[256,4096]{1,0:T(8,128)(2,1)}, u32[]{:S(2)}) copy-start(bf16[256,4096]{1,0:T(8,128)(2,1)} %param.36) | copy-start | bytes 6291460
Sparse Core Ops, SparseCore 0:
  23.4 37.7 all-reduce.3
  64.0 49.5 all-gather.1
  120.2 54.0 all-reduce.5
  176.6 37.7 reduce-scatter.2
  217.7 71.1 reduce-scatter.4
